TPU v7x, 32 devices: a whole 2x2x4 slice. The times are simulated.
32 devices in a mesh: sp: 4 (over y, core), dp: 8 (over z, x).
Axes of the slice: x: 2, y: 2, z: 4, core: 2. Of those that a mesh axis runs over, the one named last changes fastest.
Arguments:
- stream: bfloat16 [8, 512, 2064], P('dp', 'sp'), may hold values from -6 to 6
- mix_gain: float32 [2064], replicated, may hold values from 0.1 to 1.9
- query_weight: bfloat16 [2064, 2048], P('dp'), may hold values from -0.125 to 0.125
- query_gain: float32 [128], replicated, may hold values from 0.1 to 1.9
- keys: bfloat16 [8, 512, 512], P('dp', 'sp'), may hold values from -6 to 6
- key_gain: float32 [128], replicated, may hold values from 0.1 to 1.9
- values: bfloat16 [8, 512, 512], P('dp', 'sp'), may hold values from -48 to 48
- stick_offset: float32 [16], replicated, may hold values from -8.5 to -7, as said below
Outputs:
- attended: bfloat16 [8, 512, 2048], P('dp', 'sp')
Inputs may be any that keep to these rules, and one draw needn't show every extreme that they name: `stick_offset`: one offset for each query head, added to all of that head's scores.
All inputs are finite; a program needn't handle non-finite values.
Results may differ from a plain program's by a relative error of at most 0.012.
Values may be sent and summed in bfloat16 or wider, within the bound.
A program may use at most 64 MiB of HBM per device.

v0:
```python
import math
import jax
import jax.numpy as jnp
from jax import lax
from jax.sharding import PartitionSpec as P

norm_eps = 1e-06
row_block = 256
key_block = 128


def rms_scaled(inputs, gain):
    wide = inputs.astype(jnp.float32)
    scaled = wide * lax.rsqrt(jnp.mean(wide * wide, axis=-1, keepdims=True) + norm_eps) * gain
    return scaled.astype(jnp.bfloat16)


def stick_weights(scores, first_row):
    heads_here = scores.shape[0]
    rows_here = scores.shape[1]
    keys_here = scores.shape[2]
    width = math.gcd(keys_here, key_block)
    blocks_here = keys_here // width
    query_pos = first_row + jnp.arange(rows_here, dtype=jnp.int32)
    key_pos = jnp.arange(keys_here, dtype=jnp.int32)
    causal = key_pos[None, :] < query_pos[:, None]
    log_keep = jnp.where(causal, jax.nn.log_sigmoid(-scores), 0.0)
    pieces = log_keep.reshape(heads_here, rows_here, blocks_here, width)
    inner = jnp.arange(width, dtype=jnp.int32)
    upper = (inner[:, None] > inner[None, :]).astype(jnp.float32)
    local = jnp.einsum("hqbk,kj->hqbj", pieces, upper, precision=lax.Precision.HIGHEST)
    totals = jnp.sum(pieces, axis=3)
    later = lax.cumsum(totals, axis=2, reverse=True) - totals
    tail = (local + later[:, :, :, None]).reshape(heads_here, rows_here, keys_here)
    return jnp.where(causal, jnp.exp(jax.nn.log_sigmoid(scores) + tail), 0.0)


def body(stream, mix_gain, query_weight, query_gain, keys, key_gain, values, stick_offset):
    sp_count = lax.axis_size("sp")
    sp_index = lax.axis_index("sp")
    stream_rows = stream[0]
    tokens_dev = stream_rows.shape[0]
    head_width = query_gain.shape[0]
    heads_all = stick_offset.shape[0]
    heads_dev = heads_all // sp_count
    kv_count = keys.shape[2] // head_width
    group_size = sp_count // kv_count
    seq_length = tokens_dev * sp_count
    stacked = jnp.stack((keys[0], values[0]), axis=1).reshape(tokens_dev, 2, kv_count, head_width)
    copied = jnp.repeat(stacked, group_size, axis=2)
    arrived = lax.all_to_all(copied, "sp", split_axis=2, concat_axis=0, tiled=True)
    key_value = arrived[:, :, 0, :]
    normed = rms_scaled(stream_rows, mix_gain)
    columns = lax.dynamic_slice_in_dim(
        query_weight, sp_index * (heads_dev * head_width), heads_dev * head_width, 1
    )
    gathered = lax.all_gather(columns, "dp", axis=0, tiled=True)
    queries = jnp.dot(
        lax.all_gather(normed, "sp", axis=0, tiled=True),
        gathered,
        preferred_element_type=jnp.float32,
    ).astype(jnp.bfloat16)
    queries = lax.optimization_barrier(queries)
    mine = rms_scaled(queries.reshape(seq_length, heads_dev, head_width), query_gain)
    key_heads = rms_scaled(key_value[:, 0], key_gain)
    value_rows = key_value[:, 1]
    offsets = lax.dynamic_slice_in_dim(stick_offset, sp_index * heads_dev, heads_dev)
    block = math.gcd(seq_length, row_block)
    outputs = []
    for block_id in range(seq_length // block):
        first = block_id * block
        finish = first + block
        scores = jnp.einsum(
            "qhd,kd->hqk",
            mine[first:finish],
            key_heads[:finish],
            preferred_element_type=jnp.float32,
        )
        scores = scores * head_width ** (-0.5) + offsets[:, None, None]
        weights = stick_weights(scores, first).astype(jnp.bfloat16)
        outputs.append(
            jnp.einsum(
                "hqk,kd->qhd", weights, value_rows[:finish], preferred_element_type=jnp.float32
            )
        )
    attended = (
        jnp.concatenate(outputs, axis=0)
        .reshape(seq_length, heads_dev * head_width)
        .astype(jnp.bfloat16)
    )
    returned = lax.all_to_all(attended, "sp", split_axis=0, concat_axis=1, tiled=True)
    return returned[None]


def solution(mesh):
    return jax.shard_map(
        body,
        mesh=mesh,
        in_specs=(
            P("dp", "sp", None),
            P(),
            P("dp", None),
            P(),
            P("dp", "sp", None),
            P(),
            P("dp", "sp", None),
            P(),
        ),
        out_specs=P("dp", "sp", None),
        check_vma=False,
    )
```

profile of v0, /device:TPU:0, one launch (start us, length us, event | category | flops | bytes accessed | tf_op | source)
XLA Modules:
  0.0 124.1 jit_solution(3568556610034957392)
XLA Ops:
  6.5 0.0 copy-start
  6.5 0.0 copy-start.7
  6.5 0.0 copy-start.8
  6.5 0.0 all-gather.6.cloned.1.call-start
  6.6 1.2 copy-done
  7.8 0.7 dynamic-slice_bitcast_fusion
  8.5 0.0 all-gather.6.cloned.1.call-update
  8.5 0.0 copy-start.12
  8.5 0.0 all-gather.4.cloned.1.call-start
  8.6 1.3 %fusion.15 = f32[128]{0:T(128)S(1)} fusion(bf16[1,128,2064]{1,2,0:T(8,128)(2,1)} %param.8), kind=kLoop, calls=%fused_computation.31 | loop fusion | flops 792448 | bytes 528896 | tf_op jit(solution)/shard_map/reduce_sum | solution.py:14
  9.9 0.0 copy-start.10
  9.9 2.2 %fusion.17 = bf16[128,2064]{0,1:T(8,128)(2,1)} fusion(bf16[1,128,2064]{1,2,0:T(8,128)(2,1)} %param.8, f32[2064]{0:T(1024)} %param.9, f32[128]{0:T(128)S(1)} %add_rsqrt_fusion.2), kind=kLoop, calls=%fused_computation.33 | loop fusion | flops 1056768 | bytes 1065536 | tf_op jit(solution)/shard_map/convert_element_type | solution.py:15
  12.1 0.0 all-gather.4.cloned.1.call-update
  12.2 0.0 copy-done.7
  12.2 0.1 copy.54
  12.3 0.0 copy-done.8
  12.3 0.1 copy.55
  12.5 0.9 copy.56
  13.3 4.3 %all-to-all-start = ((bf16[128,2,4,128]{3,0,1,2:T(8,128)(2,1)}), bf16[128,2,4,128]{3,0,1,2:T(8,128)(2,1)S(1)}, u32[]{:S(2)}, u32[]{:S(2)}) async-start(bf16[128,2,4,128]{3,0,1,2:T(8,128)(2,1)} %copy.56), calls=%async_computation | async-start | bytes 524288 | tf_op jit(solution)/shard_map/all_to_all | solution.py:51
  17.6 0.0 copy-done.12
  17.6 0.1 dynamic_slice.7
  17.7 0.7 iota_compare_fusion
  18.5 5.2 %all-to-all-done = bf16[128,2,4,128]{3,0,1,2:T(8,128)(2,1)S(1)} async-done(((bf16[128,2,4,128]{3,0,1,2:T(8,128)(2,1)}), bf16[128,2,4,128]{3,0,1,2:T(8,128)(2,1)S(1)}, u32[]{:S(2)}, u32[]{:S(2)}) %all-to-all-start) | async-done | bytes 262176 | tf_op jit(solution)/shard_map/all_to_all | solution.py:51
  23.6 0.1 fusion.27
  23.8 0.0 copy-done.10
  23.8 0.8 fusion.29
  24.6 37.5 %all-gather.6.cloned.1.call-done = bf16[8,258,512]{2,1,0:T(8,128)(2,1)} async-done(((bf16[1,258,512]{2,1,0:T(8,128)(2,1)}), bf16[8,258,512]{2,1,0:T(8,128)(2,1)}) %all-gather.6.cloned.1.call-update) | async-done | bytes 2113552 | tf_op jit(solution)/shard_map/all_gather | solution.py:57
  62.1 1.9 %reshape.90 = bf16[2064,512]{1,0:T(8,128)(2,1)S(1)} reshape(bf16[8,258,512]{2,1,0:T(8,128)(2,1)} %all-gather.6.cloned.1.call-done) | data formatting | bytes 4227072
  63.9 21.1 %all-gather.4.cloned.1.call-done = bf16[512,2064]{0,1:T(8,128)(2,1)} async-done(((bf16[128,2064]{0,1:T(8,128)(2,1)}), bf16[512,2064]{0,1:T(8,128)(2,1)}) %all-gather.4.cloned.1.call-update) | async-done | bytes 2113552 | tf_op jit(solution)/shard_map/all_gather | solution.py:59
  85.1 3.8 %convolution_convert_fusion = bf16[512,512]{1,0:T(8,128)(2,1)} fusion(bf16[512,2064]{0,1:T(8,128)(2,1)} %all-gather.4.cloned.1.call-done, bf16[2064,512]{1,0:T(8,128)(2,1)S(1)} %reshape.90), kind=kOutput, calls=%fused_computation.26 | convolution fusion | flops 1082392576 | bytes 4751360 | tf_op jit(solution)/shard_map/dot_general | solution.py:58
  88.9 0.0 copy-start.1
  88.9 0.0 copy-start.11
  88.9 1.4 %reshape.88 = f32[512,4,128]{2,1,0:T(4,128)S(1)} reshape(bf16[512,512]{1,0:T(8,128)(2,1)} %convolution_convert_fusion) | data formatting | bytes 1572864 | tf_op jit(solution)/shard_map/convert_element_type | solution.py:13
  90.3 0.6 multiply_reduce_fusion
  90.9 0.1 copy.58
  91.1 0.0 copy-done.1
  91.1 0.0 copy-done.11
  91.1 0.3 fusion.26
  91.4 0.0 copy-start.5
  91.4 0.8 copy-done.5
  92.2 1.8 %bitcast_reduce_fusion.1 = (f32[4,256,2]{1,2,0:T(2,128)S(1)}, f32[4,256,256]{1,2,0:T(8,128)S(1)}, f32[4,256,256]{1,2,0:T(8,128)S(1)}) fusion(pred[256,256]{0,1:T(8,128)(4,1)S(1)} %iota_compare_fusion.1, f32[4]{0:T(128)S(1)} %dynamic_slice.7, bf16[512,4,128]{2,0,1:T(8,128)(2,1)S(1)} %fusion.26, bf16[512,128]{1,0:T(8,128)(2,1)} %fusion.29), kind=kOutput, calls=%fused_computation.71 | convolution fusion | flops 69990400 | bytes 2499072 | tf_op jit(solution)/shard_map/qhd,kd->hqk/dot_general | solution.py:73
  94.1 0.7 convolution_add_fusion.1
  94.7 0.0 copy-start.3
  94.7 0.0 copy-start.6
  94.8 0.0 copy-start.9
  94.8 0.8 fusion.22
  95.6 1.0 fusion.13
  96.5 0.0 copy-done.3
  96.5 0.0 copy-done.6
  96.6 0.0 copy-done.9
  96.6 3.1 %bitcast_reduce_fusion = (f32[4,256,4]{1,2,0:T(4,128)S(1)}, f32[4,256,512]{1,2,0:T(8,128)}, f32[512,256,4]{1,0,2:T(8,128)S(1)}) fusion(f32[4]{0:T(128)S(1)} %dynamic_slice.7, pred[256,512]{0,1:T(8,128)(4,1)S(1)} %copy-done.3, bf16[512,4,128]{2,0,1:T(8,128)(2,1)S(1)} %copy-done.6, bf16[512,128]{1,0:T(8,128)(2,1)S(1)} %copy-done.9), kind=kOutput, calls=%fused_computation.70 | convolution fusion | flops 139980800 | bytes 4735488 | tf_op jit(solution)/shard_map/qhd,kd->hqk/dot_general | solution.py:73
  99.6 0.1 reduce_window_sum.21
  99.7 0.0 copy-start.4
  99.7 2.9 %convolution_add_fusion = f32[4,256,4,128]{1,3,2,0:T(8,128)S(1)} fusion(f32[4,256,4,128]{1,3,2,0:T(8,128)} %bitcast.99, f32[4,256,4]{1,2,0:T(4,128)S(1)} %sub.15), kind=kOutput, calls=%fused_computation.19 | convolution fusion | flops 805847040 | bytes 4210688 | tf_op jit(solution)/shard_map/hqbk,kj->hqbj/dot_general | solution.py:31
  102.6 0.0 copy-done.4
  102.6 0.0 copy-start.2
  102.6 1.8 %fusion.4 = bf16[4,256,512]{1,2,0:T(8,128)(2,1)S(1)} fusion(f32[4,256,4,128]{1,3,2,0:T(8,128)S(1)} %convolution_add_fusion, f32[512,256,4]{1,0,2:T(8,128)S(1)} %get-tuple-element.9, f32[4]{0:T(128)S(1)} %dynamic_slice.7, pred[256,512]{0,1:T(8,128)(4,1)S(1)} %copy-done.4), kind=kLoop, calls=%fused_computation.8 | loop fusion | flops 6815744 | bytes 5373968 | tf_op jit(solution)/shard_map/convert_element_type | solution.py:80
  104.4 0.3 fusion.14
  104.7 0.0 copy-done.2
  104.8 0.1 convert_element_type.55
  104.9 0.1 copy.66
  105.0 11.2 %all_to_all.28 = bf16[4,128,512]{1,2,0:T(8,128)(2,1)S(1)} all-to-all(bf16[4,128,512]{1,2,0:T(8,128)(2,1)S(1)} %copy.66), channel_id=1, replica_groups=mesh['sp'=4,'dp'=8] {'sp'}, dimensions={0} | all-to-all | bytes 1048576 | tf_op jit(solution)/shard_map/all_to_all | solution.py:91
  116.2 1.0 copy.67
  (11 shorter events, 0.2 us)
Async XLA Ops:
  6.5 1.2 copy-start
  6.5 5.6 %copy-start.7 = (bf16[1,128,512]{2,1,0:T(8,128)(2,1)S(1)}, bf16[1,128,512]{2,1,0:T(8,128)(2,1)}, u32[]{:S(2)}) copy-start(bf16[1,128,512]{2,1,0:T(8,128)(2,1)} %param.12) | copy-start | bytes 393220
  6.5 5.8 %copy-start.8 = (bf16[1,128,512]{2,1,0:T(8,128)(2,1)S(1)}, bf16[1,128,512]{2,1,0:T(8,128)(2,1)}, u32[]{:S(2)}) copy-start(bf16[1,128,512]{2,1,0:T(8,128)(2,1)} %param.14) | copy-start | bytes 393220
  6.5 55.5 %all-gather.6.cloned.1.call-start = ((), (), s32[]{:S(2)}) async-start(), calls=%async_computation.3 | async-start | bytes 2433024 | tf_op jit(solution)/shard_map/all_gather | solution.py:57
  8.5 9.1 %copy-start.12 = (f32[16]{0:T(128)S(1)}, f32[16]{0:T(128)}, u32[]{:S(2)}) copy-start(f32[16]{0:T(128)} %param.15) | copy-start | bytes 196
  8.5 76.5 %all-gather.4.cloned.1.call-start = ((), (), s32[]{:S(2)}) async-start(), calls=%async_computation.2 | async-start | bytes 2641920 | tf_op jit(solution)/shard_map/all_gather | solution.py:59
  9.9 13.9 %copy-start.10 = (f32[128]{0:T(128)S(1)}, f32[128]{0:T(128)}, u32[]{:S(2)}) copy-start(f32[128]{0:T(128)} %param.13) | copy-start | bytes 1540
  13.3 10.3 %all-to-all-start = ((bf16[128,2,4,128]{3,0,1,2:T(8,128)(2,1)}), bf16[128,2,4,128]{3,0,1,2:T(8,128)(2,1)S(1)}, u32[]{:S(2)}, u32[]{:S(2)}) async-start(bf16[128,2,4,128]{3,0,1,2:T(8,128)(2,1)} %copy.56), calls=%async_computation | async-start | bytes 524288 | tf_op jit(solution)/shard_map/all_to_all | solution.py:51
  88.9 2.2 %copy-start.1 = (bf16[512,512]{1,0:T(8,128)(2,1)S(1)}, bf16[512,512]{1,0:T(8,128)(2,1)}, u32[]{:S(2)}) copy-start(bf16[512,512]{1,0:T(8,128)(2,1)} %convolution_convert_fusion) | copy-start | bytes 1572868
  88.9 2.2 %copy-start.11 = (f32[128]{0:T(128)S(1)}, f32[128]{0:T(128)}, u32[]{:S(2)}) copy-start(f32[128]{0:T(128)} %param.11) | copy-start | bytes 1540
  91.4 0.8 copy-start.5
  94.7 1.8 %copy-start.3 = (pred[256,512]{0,1:T(8,128)(4,1)S(1)}, pred[256,512]{0,1:T(8,128)(4,1)}, u32[]{:S(2)}) copy-start(pred[256,512]{0,1:T(8,128)(4,1)} %iota_compare_fusion) | copy-start | bytes 393220
  94.7 1.8 %copy-start.6 = (bf16[512,4,128]{2,0,1:T(8,128)(2,1)S(1)}, bf16[512,4,128]{2,0,1:T(8,128)(2,1)}, u32[]{:S(2)}) copy-start(bf16[512,4,128]{2,0,1:T(8,128)(2,1)} %copy-done.5) | copy-start | bytes 1572868
  94.8 1.8 %copy-start.9 = (bf16[512,128]{1,0:T(8,128)(2,1)S(1)}, bf16[512,128]{1,0:T(8,128)(2,1)}, u32[]{:S(2)}) copy-start(bf16[512,128]{1,0:T(8,128)(2,1)} %fusion.29) | copy-start | bytes 393220
  99.7 2.9 %copy-start.4 = (pred[256,512]{0,1:T(8,128)(4,1)S(1)}, pred[256,512]{0,1:T(8,128)(4,1)}, u32[]{:S(2)}) copy-start(pred[256,512]{0,1:T(8,128)(4,1)} %iota_compare_fusion) | copy-start | bytes 393220
  102.6 2.1 %copy-start.2 = (bf16[256,4,128]{0,2,1:T(8,128)(2,1)S(1)}, bf16[256,4,128]{0,2,1:T(8,128)(2,1)}, u32[]{:S(2)}) copy-start(bf16[256,4,128]{0,2,1:T(8,128)(2,1)} %fusion.13) | copy-start | bytes 786436
Sparse Core Ops, SparseCore 0:
  9.5 52.5 all-gather.5
  63.6 21.4 all-gather.3
where the time goes:
time: 125 us; the launch traced here: 124 us
  waiting for transfers between devices  63.8 us (51%)
  between operations  13.7 us (11%)
  matrix products  13.5 us (11%)
  blocking collectives  11.2 us (9%)
  other arithmetic  9.01 us (7%)
  local copies, waits for them, and re-layouts  8.58 us (7%)
  starting transfers between devices  4.31 us (3%)
    all_gather x1, waiting for transfers between devices, body(): gathered = lax.all_gather(columns, 'dp', axis=0, tiled=True)  37.5 us
    all_gather x1, waiting for transfers between devices, body(): lax.all_gather(normed, 'sp', axis=0, tiled=True)  21.1 us
    all_to_all x1, blocking collectives, body(): lax.all_to_all(attended, 'sp', split_axis=0, concat_axis=1, tiled=True)  11.2 us
    all_to_all x1, waiting for transfers between devices, body(): lax.all_to_all(copied, 'sp', split_axis=2, concat_axis=0, tiled=True)  5.16 us
    unnamed x30, local copies, waits for them, and re-layouts  4.87 us
    dot_general x2, matrix products, body(): jnp.einsum('qhd,kd->hqk', mine[first:finish], key_heads[:finish], preferr...  4.85 us
    all_to_all x1, starting transfers between devices, body(): lax.all_to_all(copied, 'sp', split_axis=2, concat_axis=0, tiled=True)  4.26 us
    dot_general x1, matrix products, body(): jnp.dot(lax.all_gather(normed, 'sp', axis=0, tiled=True), gathered, prefe...  3.8 us
  transfers between devices with their start and end apart: 3, of which 3 were waited for; matrix products, arithmetic and copies ran while one was open for 7% of the time, Pallas kernels for 0%

commit v1 on v0

--- a/solution.py
+++ b/solution.py
@@ -54,7 +54,18 @@
     columns = lax.dynamic_slice_in_dim(
         query_weight, sp_index * (heads_dev * head_width), heads_dev * head_width, 1
     )
-    gathered = lax.all_gather(columns, "dp", axis=0, tiled=True)
+    n_axis = lax.axis_size("dp")
+    latest = sorted(((to_i, (to_i + 1) % n_axis) for to_i in range(n_axis)))
+    big = columns
+    c = 1
+    runs = [big]
+    while c < n_axis:
+        big = lax.ppermute(big, "dp", latest)
+        runs.insert(0, big)
+        c += 1
+    w2 = jnp.concatenate(runs, axis=0)
+    new = lax.axis_index("dp") + 1
+    gathered = jnp.roll(w2, new * columns.shape[0], axis=0)
     queries = jnp.dot(
         lax.all_gather(normed, "sp", axis=0, tiled=True),
         gathered,

time: 125 us -> 152 us (1.22)
  local copies, waits for them, and re-layouts: 8.58 us -> 38 us
  waiting for transfers between devices: 63.8 us -> 58.1 us
  starting transfers between devices: 4.31 us -> 7.07 us
    ppermute x0 -> x7, waiting for transfers between devices: none -> 56.9 us  [body(): big = lax.ppermute(big, 'dp', latest)]
    all_gather x1 -> x0, waiting for transfers between devices: 37.5 us -> none  [body(): gathered = lax.all_gather(columns, 'dp', axis=0, tiled=True)]
    concatenate x0 -> x1, local copies, waits for them, and re-layouts: none -> 33.4 us  [body(): gathered = jnp.roll(w2, new * columns.shape[0], axis=0)]
    all_gather x1, waiting for transfers between devices: 21.1 us -> 0.01 us  [body(): lax.all_gather(normed, 'sp', axis=0, tiled=True)]
    all_to_all x1, waiting for transfers between devices: 5.16 us -> 1.26 us  [body(): lax.all_to_all(copied, 'sp', split_axis=2, concat_axis=0, tiled=True)]
    unnamed x30 -> x26, local copies, waits for them, and re-layouts: 4.87 us -> 1.07 us
    ppermute x0 -> x7, starting transfers between devices: none -> 3.04 us  [body(): big = lax.ppermute(big, 'dp', latest)]
  transfers between devices with their start and end apart: 3 -> 9, of which waited for: 3 -> 8; matrix products, arithmetic and copies ran while one was open for 7% -> 25% of each run, Pallas kernels for 0% -> 0%
where the time goes in v1:
time: 152 us; the launch traced here: 151 us
  waiting for transfers between devices  58.1 us (38%)
  local copies, waits for them, and re-layouts  38 us (25%)
  between operations  13.7 us (9%)
  matrix products  13.3 us (9%)
  blocking collectives  11.2 us (7%)
  other arithmetic  9.08 us (6%)
  starting transfers between devices  7.07 us (5%)
    ppermute x7, waiting for transfers between devices, body(): big = lax.ppermute(big, 'dp', latest)  56.9 us
    concatenate x1, local copies, waits for them, and re-layouts, body(): gathered = jnp.roll(w2, new * columns.shape[0], axis=0)  33.4 us
    all_to_all x1, blocking collectives, body(): lax.all_to_all(attended, 'sp', split_axis=0, concat_axis=1, tiled=True)  11.2 us
    dot_general x2, matrix products, body(): jnp.einsum('qhd,kd->hqk', mine[first:finish], key_heads[:finish], preferr...  4.84 us
    all_to_all x1, starting transfers between devices, body(): lax.all_to_all(copied, 'sp', split_axis=2, concat_axis=0, tiled=True)  4.03 us
    dot_general x1, matrix products, body(): jnp.dot(lax.all_gather(normed, 'sp', axis=0, tiled=True), gathered, prefe...  3.65 us
    dot_general x2, matrix products, stick_weights(): jnp.einsum('hqbk,kj->hqbj', pieces, upper, precision=lax.Precision.HIGHEST)  3.53 us
    convert_element_type x3, other arithmetic, rms_scaled(): return scaled.astype(jnp.bfloat16)  3.34 us
  transfers between devices with their start and end apart: 9, of which 8 were waited for; matrix products, arithmetic and copies ran while one was open for 25% of the time, Pallas kernels for 0%

profile of v1, /device:TPU:0, one launch (start us, length us, event | category | flops | bytes accessed | tf_op | source)
XLA Modules:
  0.0 150.5 jit_solution(10587345647000402010)
XLA Ops:
  6.5 0.0 copy-start
  6.5 0.0 all-gather.2.cloned.1.call-start
  6.5 1.4 fusion.20
  8.0 2.2 %fusion.22 = bf16[128,2064]{0,1:T(8,128)(2,1)} fusion(bf16[1,128,2064]{1,2,0:T(8,128)(2,1)} %param.8, f32[2064]{0:T(1024)} %param.9, f32[128]{0:T(128)S(1)} %add_rsqrt_fusion.2), kind=kLoop, calls=%fused_computation.35 | loop fusion | flops 1056768 | bytes 1065536 | tf_op jit(solution)/shard_map/convert_element_type | solution.py:15
  10.2 0.0 all-gather.2.cloned.1.call-update
  10.2 0.0 copy-done
  10.3 3.0 %collective-permute-start = (bf16[258,512]{1,0:T(8,128)(2,1)S(1)}, bf16[258,512]{1,0:T(8,128)(2,1)S(1)}, u32[]{:S(2)}, u32[]{:S(2)}) collective-permute-start(bf16[258,512]{1,0:T(8,128)(2,1)S(1)} %constant_dynamic-slice_fusion), channel_id=1, source_target_pairs={{0,1},{1,2},{2,3},{3,4},{4,5},{5,6},{6,7},{7,0},{8,9},{9,10},{10,1... | collective-permute-start | bytes 792584 | tf_op jit(solution)/shard_map/ppermute | solution.py:63
  13.3 9.5 %collective-permute-done = bf16[258,512]{1,0:T(8,128)(2,1)S(1)} collective-permute-done((bf16[258,512]{1,0:T(8,128)(2,1)S(1)}, bf16[258,512]{1,0:T(8,128)(2,1)S(1)}, u32[]{:S(2)}, u32[]{:S(2)}) %collective-permute-start) | collective-permute-done | bytes 264224 | tf_op jit(solution)/shard_map/ppermute | solution.py:63
  22.8 0.0 collective-permute-start.1
  22.8 10.3 %collective-permute-done.1 = bf16[258,512]{1,0:T(8,128)(2,1)S(1)} collective-permute-done((bf16[258,512]{1,0:T(8,128)(2,1)S(1)}, bf16[258,512]{1,0:T(8,128)(2,1)S(1)}, u32[]{:S(2)}, u32[]{:S(2)}) %collective-permute-start.1) | collective-permute-done | bytes 264224 | tf_op jit(solution)/shard_map/ppermute | solution.py:63
  33.2 0.0 collective-permute-start.2
  33.2 9.5 %collective-permute-done.2 = bf16[258,512]{1,0:T(8,128)(2,1)S(1)} collective-permute-done((bf16[258,512]{1,0:T(8,128)(2,1)S(1)}, bf16[258,512]{1,0:T(8,128)(2,1)S(1)}, u32[]{:S(2)}, u32[]{:S(2)}) %collective-permute-start.2) | collective-permute-done | bytes 264224 | tf_op jit(solution)/shard_map/ppermute | solution.py:63
  42.7 0.0 collective-permute-start.3
  42.7 9.2 %collective-permute-done.3 = bf16[258,512]{1,0:T(8,128)(2,1)S(1)} collective-permute-done((bf16[258,512]{1,0:T(8,128)(2,1)S(1)}, bf16[258,512]{1,0:T(8,128)(2,1)S(1)}, u32[]{:S(2)}, u32[]{:S(2)}) %collective-permute-start.3) | collective-permute-done | bytes 264224 | tf_op jit(solution)/shard_map/ppermute | solution.py:63
  51.8 0.0 collective-permute-start.4
  51.8 0.0 copy-done.6
  51.8 0.1 copy.44
  51.9 0.0 copy-done.7
  52.0 0.1 copy.45
  52.1 0.8 copy.46
  53.0 4.0 %all-to-all-start = ((bf16[128,2,4,128]{3,0,1,2:T(8,128)(2,1)}), bf16[128,2,4,128]{3,0,1,2:T(8,128)(2,1)}, u32[]{:S(2)}, u32[]{:S(2)}) async-start(bf16[128,2,4,128]{3,0,1,2:T(8,128)(2,1)} %copy.46), calls=%async_computation | async-start | bytes 524288 | tf_op jit(solution)/shard_map/all_to_all | solution.py:51
  57.0 4.0 %collective-permute-done.4 = bf16[258,512]{1,0:T(8,128)(2,1)S(1)} collective-permute-done((bf16[258,512]{1,0:T(8,128)(2,1)S(1)}, bf16[258,512]{1,0:T(8,128)(2,1)S(1)}, u32[]{:S(2)}, u32[]{:S(2)}) %collective-permute-start.4) | collective-permute-done | bytes 264224 | tf_op jit(solution)/shard_map/ppermute | solution.py:63
  61.0 0.0 collective-permute-start.5
  61.0 0.7 iota_compare_fusion
  61.7 0.0 copy-done.11
  61.7 0.1 dynamic_slice.12
  61.8 1.3 all-to-all-done
  63.1 1.0 copy.47
  64.0 0.1 fusion.32
  64.2 5.9 %collective-permute-done.5 = bf16[258,512]{1,0:T(8,128)(2,1)S(1)} collective-permute-done((bf16[258,512]{1,0:T(8,128)(2,1)S(1)}, bf16[258,512]{1,0:T(8,128)(2,1)S(1)}, u32[]{:S(2)}, u32[]{:S(2)}) %collective-permute-start.5) | collective-permute-done | bytes 264224 | tf_op jit(solution)/shard_map/ppermute | solution.py:63
  70.1 0.0 collective-permute-start.6
  70.1 0.0 copy-done.9
  70.1 0.8 fusion.34
  70.9 8.5 %collective-permute-done.6 = bf16[258,512]{1,0:T(8,128)(2,1)} collective-permute-done((bf16[258,512]{1,0:T(8,128)(2,1)S(1)}, bf16[258,512]{1,0:T(8,128)(2,1)}, u32[]{:S(2)}, u32[]{:S(2)}) %collective-permute-start.6) | collective-permute-done | bytes 264224 | tf_op jit(solution)/shard_map/ppermute | solution.py:63
  79.4 33.4 %concatenate.11 = bf16[4128,512]{1,0:T(8,128)(2,1)} concatenate(bf16[258,512]{1,0:T(8,128)(2,1)} %collective-permute-done.6, bf16[258,512]{1,0:T(8,128)(2,1)S(1)} %collective-permute-done.5, bf16[258,512]{1,0:T(8,128)(2,1)S(1)} %collective-permute-done.4, bf16[258,512]{1,0:T(8,128)(2,1)S(1)} %collective-permute-done.3, bf16[258,512]{1,0:T(8,128)(2,1)S(1)} %collective-permute-done.2, ...), dimensions={0} | concatenate | bytes 8454144 | tf_op jit(solution)/shard_map/jit(_roll_dynamic)/concatenate | solution.py:68
  112.8 3.7 %fusion.15 = bf16[512,512]{1,0:T(8,128)(2,1)S(1)} fusion(bf16[512,2064]{0,1:T(8,128)(2,1)} %all-gather.2.cloned.1.call-done, bf16[4128,512]{1,0:T(8,128)(2,1)} %concatenate.11, s32[]{:T(128)S(6)} %select_n.51), kind=kOutput, calls=%fused_computation.28 | convolution fusion | flops 1082392576 | bytes 4751364 | tf_op jit(solution)/shard_map/dot_general | solution.py:69
  116.5 0.0 copy-start.10
  116.5 0.3 reshape.88
  116.8 0.6 multiply_reduce_fusion
  117.4 0.1 copy.48
  117.6 0.0 copy-done.10
  117.6 0.3 fusion.31
  117.9 0.0 copy-start.4
  117.9 0.8 copy-done.4
  118.7 1.8 %bitcast_reduce_fusion.1 = (f32[4,256,2]{1,2,0:T(2,128)S(1)}, f32[4,256,256]{1,2,0:T(8,128)S(1)}, f32[4,256,256]{1,2,0:T(8,128)S(1)}) fusion(pred[256,256]{0,1:T(8,128)(4,1)S(1)} %iota_compare_fusion.1, f32[4]{0:T(128)S(1)} %dynamic_slice.12, bf16[512,4,128]{2,0,1:T(8,128)(2,1)S(1)} %fusion.31, bf16[512,128]{1,0:T(8,128)(2,1)} %fusion.34), kind=kOutput, calls=%fused_computation.74 | convolution fusion | flops 69990400 | bytes 2499072 | tf_op jit(solution)/shard_map/qhd,kd->hqk/dot_general | solution.py:84
  120.5 0.7 convolution_add_fusion.1
  121.2 0.0 copy-start.2
  121.2 0.0 copy-start.5
  121.2 0.0 copy-start.8
  121.2 0.8 fusion.27
  122.0 1.0 fusion.18
  123.0 0.0 copy-done.2
  123.0 0.0 copy-done.5
  123.0 0.0 copy-done.8
  123.0 3.1 %bitcast_reduce_fusion = (f32[4,256,4]{1,2,0:T(4,128)S(1)}, f32[4,256,512]{1,2,0:T(8,128)}, f32[512,256,4]{1,0,2:T(8,128)S(1)}) fusion(f32[4]{0:T(128)S(1)} %dynamic_slice.12, pred[256,512]{0,1:T(8,128)(4,1)S(1)} %copy-done.2, bf16[512,4,128]{2,0,1:T(8,128)(2,1)S(1)} %copy-done.5, bf16[512,128]{1,0:T(8,128)(2,1)S(1)} %copy-done.8), kind=kOutput, calls=%fused_computation.73 | convolution fusion | flops 139980800 | bytes 4735488 | tf_op jit(solution)/shard_map/qhd,kd->hqk/dot_general | solution.py:84
  126.1 0.1 reduce_window_sum.21
  126.1 0.0 copy-start.3
  126.2 2.9 %convolution_add_fusion = f32[4,256,4,128]{1,3,2,0:T(8,128)S(1)} fusion(f32[4,256,4,128]{1,3,2,0:T(8,128)} %bitcast.96, f32[4,256,4]{1,2,0:T(4,128)S(1)} %sub.20), kind=kOutput, calls=%fused_computation.21 | convolution fusion | flops 805847040 | bytes 4210688 | tf_op jit(solution)/shard_map/hqbk,kj->hqbj/dot_general | solution.py:31
  129.1 1.8 %fusion.6 = bf16[4,256,512]{1,2,0:T(8,128)(2,1)S(1)} fusion(f32[4,256,4,128]{1,3,2,0:T(8,128)S(1)} %convolution_add_fusion, f32[512,256,4]{1,0,2:T(8,128)S(1)} %get-tuple-element.9, f32[4]{0:T(128)S(1)} %dynamic_slice.12, pred[256,512]{0,1:T(8,128)(4,1)S(1)} %copy-done.3), kind=kLoop, calls=%fused_computation.10 | loop fusion | flops 6815744 | bytes 5373968 | tf_op jit(solution)/shard_map/convert_element_type | solution.py:91
  130.9 0.3 fusion.19
  131.2 0.1 convert_element_type.55
  131.4 0.1 copy.56
  131.5 11.2 %all_to_all.28 = bf16[4,128,512]{1,2,0:T(8,128)(2,1)S(1)} all-to-all(bf16[4,128,512]{1,2,0:T(8,128)(2,1)S(1)} %copy.56), channel_id=1, replica_groups=mesh['sp'=4,'dp'=8] {'sp'}, dimensions={0} | all-to-all | bytes 1048576 | tf_op jit(solution)/shard_map/all_to_all | solution.py:102
  142.7 1.0 copy.57
  (19 shorter events, 0.2 us)
Async XLA Ops:
  6.5 3.7 %copy-start = (bf16[258,2048]{1,0:T(8,128)(2,1)S(1)}, bf16[258,2048]{1,0:T(8,128)(2,1)}, u32[]{:S(2)}) copy-start(bf16[258,2048]{1,0:T(8,128)(2,1)} %param.10) | copy-start | bytes 3170308
  6.5 45.3 %copy-start.6 = (bf16[1,128,512]{2,1,0:T(8,128)(2,1)S(1)}, bf16[1,128,512]{2,1,0:T(8,128)(2,1)}, u32[]{:S(2)}) copy-start(bf16[1,128,512]{2,1,0:T(8,128)(2,1)} %param.12) | copy-start | bytes 393220
  6.5 45.4 %copy-start.7 = (bf16[1,128,512]{2,1,0:T(8,128)(2,1)S(1)}, bf16[1,128,512]{2,1,0:T(8,128)(2,1)}, u32[]{:S(2)}) copy-start(bf16[1,128,512]{2,1,0:T(8,128)(2,1)} %param.14) | copy-start | bytes 393220
  6.5 106.3 %all-gather.2.cloned.1.call-start = ((), (), s32[]{:S(2)}) async-start(), calls=%async_computation.2 | async-start | bytes 2641920 | tf_op jit(solution)/shard_map/all_gather | solution.py:70
  8.0 53.7 %copy-start.11 = (f32[16]{0:T(128)S(1)}, f32[16]{0:T(128)}, u32[]{:S(2)}) copy-start(f32[16]{0:T(128)} %param.15) | copy-start | bytes 196
  10.2 59.9 %copy-start.9 = (f32[128]{0:T(128)S(1)}, f32[128]{0:T(128)}, u32[]{:S(2)}) copy-start(f32[128]{0:T(128)} %param.13) | copy-start | bytes 1540
  10.3 12.5 %collective-permute-start = (bf16[258,512]{1,0:T(8,128)(2,1)S(1)}, bf16[258,512]{1,0:T(8,128)(2,1)S(1)}, u32[]{:S(2)}, u32[]{:S(2)}) collective-permute-start(bf16[258,512]{1,0:T(8,128)(2,1)S(1)} %constant_dynamic-slice_fusion), channel_id=1, source_target_pairs={{0,1},{1,2},{2,3},{3,4},{4,5},{5,6},{6,7},{7,0},{8,9},{9,10},{10,1... | collective-permute-start | bytes 792584 | tf_op jit(solution)/shard_map/ppermute | solution.py:63
  22.8 10.3 %collective-permute-start.1 = (bf16[258,512]{1,0:T(8,128)(2,1)S(1)}, bf16[258,512]{1,0:T(8,128)(2,1)S(1)}, u32[]{:S(2)}, u32[]{:S(2)}) collective-permute-start(bf16[258,512]{1,0:T(8,128)(2,1)S(1)} %collective-permute-done), channel_id=1, source_target_pairs={{0,1},{1,2},{2,3},{3,4},{4,5},{5,6},{6,7},{7,0},{8,9},{9,10},{10,1... | collective-permute-start | bytes 792584 | tf_op jit(solution)/shard_map/ppermute | solution.py:63
  33.2 9.5 %collective-permute-start.2 = (bf16[258,512]{1,0:T(8,128)(2,1)S(1)}, bf16[258,512]{1,0:T(8,128)(2,1)S(1)}, u32[]{:S(2)}, u32[]{:S(2)}) collective-permute-start(bf16[258,512]{1,0:T(8,128)(2,1)S(1)} %collective-permute-done.1), channel_id=1, source_target_pairs={{0,1},{1,2},{2,3},{3,4},{4,5},{5,6},{6,7},{7,0},{8,9},{9,10},{10,1... | collective-permute-start | bytes 792584 | tf_op jit(solution)/shard_map/ppermute | solution.py:63
  42.7 9.2 %collective-permute-start.3 = (bf16[258,512]{1,0:T(8,128)(2,1)S(1)}, bf16[258,512]{1,0:T(8,128)(2,1)S(1)}, u32[]{:S(2)}, u32[]{:S(2)}) collective-permute-start(bf16[258,512]{1,0:T(8,128)(2,1)S(1)} %collective-permute-done.2), channel_id=1, source_target_pairs={{0,1},{1,2},{2,3},{3,4},{4,5},{5,6},{6,7},{7,0},{8,9},{9,10},{10,1... | collective-permute-start | bytes 792584 | tf_op jit(solution)/shard_map/ppermute | solution.py:63
  51.8 9.2 %collective-permute-start.4 = (bf16[258,512]{1,0:T(8,128)(2,1)S(1)}, bf16[258,512]{1,0:T(8,128)(2,1)S(1)}, u32[]{:S(2)}, u32[]{:S(2)}) collective-permute-start(bf16[258,512]{1,0:T(8,128)(2,1)S(1)} %collective-permute-done.3), channel_id=1, source_target_pairs={{0,1},{1,2},{2,3},{3,4},{4,5},{5,6},{6,7},{7,0},{8,9},{9,10},{10,1... | collective-permute-start | bytes 792584 | tf_op jit(solution)/shard_map/ppermute | solution.py:63
  53.0 10.1 %all-to-all-start = ((bf16[128,2,4,128]{3,0,1,2:T(8,128)(2,1)}), bf16[128,2,4,128]{3,0,1,2:T(8,128)(2,1)}, u32[]{:S(2)}, u32[]{:S(2)}) async-start(bf16[128,2,4,128]{3,0,1,2:T(8,128)(2,1)} %copy.46), calls=%async_computation | async-start | bytes 524288 | tf_op jit(solution)/shard_map/all_to_all | solution.py:51
  61.0 9.2 %collective-permute-start.5 = (bf16[258,512]{1,0:T(8,128)(2,1)S(1)}, bf16[258,512]{1,0:T(8,128)(2,1)S(1)}, u32[]{:S(2)}, u32[]{:S(2)}) collective-permute-start(bf16[258,512]{1,0:T(8,128)(2,1)S(1)} %collective-permute-done.4), channel_id=1, source_target_pairs={{0,1},{1,2},{2,3},{3,4},{4,5},{5,6},{6,7},{7,0},{8,9},{9,10},{10,1... | collective-permute-start | bytes 792584 | tf_op jit(solution)/shard_map/ppermute | solution.py:63
  70.1 9.3 %collective-permute-start.6 = (bf16[258,512]{1,0:T(8,128)(2,1)S(1)}, bf16[258,512]{1,0:T(8,128)(2,1)}, u32[]{:S(2)}, u32[]{:S(2)}) collective-permute-start(bf16[258,512]{1,0:T(8,128)(2,1)S(1)} %collective-permute-done.5), channel_id=1, source_target_pairs={{0,1},{1,2},{2,3},{3,4},{4,5},{5,6},{6,7},{7,0},{8,9},{9,10},{10,1... | collective-permute-start | bytes 792584 | tf_op jit(solution)/shard_map/ppermute | solution.py:63
  116.5 1.1 copy-start.10
  117.9 0.8 copy-start.4
  121.2 1.8 %copy-start.2 = (pred[256,512]{0,1:T(8,128)(4,1)S(1)}, pred[256,512]{0,1:T(8,128)(4,1)}, u32[]{:S(2)}) copy-start(pred[256,512]{0,1:T(8,128)(4,1)} %iota_compare_fusion) | copy-start | bytes 393220
  121.2 1.8 %copy-start.5 = (bf16[512,4,128]{2,0,1:T(8,128)(2,1)S(1)}, bf16[512,4,128]{2,0,1:T(8,128)(2,1)}, u32[]{:S(2)}) copy-start(bf16[512,4,128]{2,0,1:T(8,128)(2,1)} %copy-done.4) | copy-start | bytes 1572868
  121.2 1.8 %copy-start.8 = (bf16[512,128]{1,0:T(8,128)(2,1)S(1)}, bf16[512,128]{1,0:T(8,128)(2,1)}, u32[]{:S(2)}) copy-start(bf16[512,128]{1,0:T(8,128)(2,1)} %fusion.34) | copy-start | bytes 393220
  126.1 2.9 %copy-start.3 = (pred[256,512]{0,1:T(8,128)(4,1)S(1)}, pred[256,512]{0,1:T(8,128)(4,1)}, u32[]{:S(2)}) copy-start(pred[256,512]{0,1:T(8,128)(4,1)} %iota_compare_fusion) | copy-start | bytes 393220
  129.0 2.1 %copy-start.1 = (bf16[256,4,128]{0,2,1:T(8,128)(2,1)S(1)}, bf16[256,4,128]{0,2,1:T(8,128)(2,1)}, u32[]{:S(2)}) copy-start(bf16[256,4,128]{0,2,1:T(8,128)(2,1)} %fusion.18) | copy-start | bytes 786436
Sparse Core Ops, SparseCore 0:
  10.4 25.6 all-gather.1
